TPU v7x, 128 devices: a whole 4x4x4 slice. The times are simulated.
128 devices in a mesh: fs: 16 (over z, x), tp: 8 (over y, core).
Axes of the slice: x: 4, y: 4, z: 4, core: 2. Of those that a mesh axis runs over, the one named last changes fastest.
Arguments:
- normed_input: bfloat16 [32768, 2048], P('fs'), may hold values from -6 to 6
- forget_cot: bfloat16 [32768, 2048], P('fs', 'tp'), may hold values from -6 to 6
- value_cot: bfloat16 [32768, 2048], P('fs', 'tp'), may hold values from -6 to 6
- gated_output: bfloat16 [32768, 2048], P('fs', 'tp'), may hold values from -6 to 6
- output_cot: bfloat16 [32768, 2048], P('fs'), may hold values from -6 to 6
- forget_weight: float32 [2048, 2048], P('fs', 'tp'), may hold values from -0.125 to 0.125
- value_weight: float32 [2048, 2048], P('fs', 'tp'), may hold values from -0.125 to 0.125
- out_weight: float32 [2048, 2048], P('tp', 'fs'), may hold values from -0.125 to 0.125
- bases: bfloat16 [3, 2048, 256], replicated, may hold values from -0.125 to 0.125
- first_moment: float32 [256, 3, 2048], P('fs', None, 'tp'), may hold values from -4 to 4
- second_moment: float32 [256, 3, 2048], P('fs', None, 'tp'), may hold values from 0.25 to 4
Outputs:
- new_forget: float32 [2048, 2048], P('fs', 'tp')
- new_value: float32 [2048, 2048], P('fs', 'tp')
- new_out: float32 [2048, 2048], P('tp', 'fs')
- copy_forget: bfloat16 [2048, 2048], P(None, 'tp')
- copy_value: bfloat16 [2048, 2048], P(None, 'tp')
- copy_out: bfloat16 [2048, 2048], P('tp')
- moment_one: float32 [256, 3, 2048], P('fs', None, 'tp')
- moment_two: float32 [256, 3, 2048], P('fs', None, 'tp')
- step_forget: float32 [2048, 2048], P('fs', 'tp')
- step_value: float32 [2048, 2048], P('fs', 'tp')
- step_out: float32 [2048, 2048], P('tp', 'fs')
All inputs are finite; a program needn't handle non-finite values.
Results may differ from a plain program's by a relative error of at most 0.0045.
Values may be sent and summed in bfloat16 or wider, within the bound.
A program may use at most 128 MiB of HBM per device.

v0:
```python
import functools

import jax
import jax.numpy as jnp
from jax import lax
from jax.sharding import Mesh
from jax.sharding import PartitionSpec as P

FS = ("fs_0", "fs_1")
FS_TP = ("fs_0", "fs_1", "tp_0", "tp_1")
TP = ("tp_0", "tp_1")


def in_blocks(value, dim, count):
    before, after = (value.shape[:dim], value.shape[dim + 1 :])
    return jnp.moveaxis(value.reshape(*before, count, -1, *after), dim, 0)


def sum_at_owner(value, axis, dim):
    pieces = in_blocks(value, dim, lax.axis_size(axis))
    arrived = lax.all_to_all(pieces, axis, split_axis=0, concat_axis=0, tiled=True)
    return arrived.astype(jnp.float32).sum(axis=0)


def joined_along(pieces, dim):
    dims = list(pieces.shape[1:])
    dims[dim] *= pieces.shape[0]
    return jnp.moveaxis(pieces, 0, dim).reshape(dims)


def sent_to_all(value, axis):
    copies = jnp.broadcast_to(value, (lax.axis_size(axis), *value.shape))
    return lax.all_to_all(copies, axis, split_axis=0, concat_axis=0, tiled=True)


def gather_directly(value, axis, dim):
    return joined_along(sent_to_all(value, axis), dim)


def over_axes(value, axes):
    return functools.reduce(lax.psum, axes, value)


def gather_turned(arrays, axis, dims):
    turned = [jnp.moveaxis(a, dim, 0) for a, dim in zip(arrays, dims)]
    both = jnp.concatenate([t.reshape(len(t), -1) for t in turned], axis=1)
    result, at, finished = (lax.all_gather(both, axis, axis=0, tiled=True), 0, [])
    for t, dim in zip(turned, dims):
        piece = result[:, at : at + t[0].size].reshape(-1, *t.shape[1:])
        finished.append(jnp.moveaxis(piece, 0, dim))
        at += t[0].size
    return tuple(finished)


def split_parts(values):
    high = lax.optimization_barrier(values.astype(jnp.bfloat16))
    low = (values - high.astype(jnp.float32)).astype(jnp.bfloat16)
    return (high, low)


def on_device(
    normed_input,
    forget_cot,
    value_cot,
    gated_output,
    output_cot,
    forget_weight,
    value_weight,
    out_weight,
    bases,
    first_moment,
    second_moment,
):
    rows = forget_weight.shape[0]
    rank_rows = first_moment.shape[0]
    columns = forget_weight.shape[1]
    offset = lax.axis_index(FS) * rows
    factor = float(normed_input.shape[0] * lax.axis_size(FS)) ** (-0.5)
    my_bases = lax.dynamic_slice_in_dim(bases, offset, rows, 1)
    reduced = jnp.stack(
        [
            jnp.dot(normed_input, bases[0], preferred_element_type=jnp.float32),
            jnp.dot(normed_input, bases[1], preferred_element_type=jnp.float32),
            jnp.dot(output_cot, bases[2], preferred_element_type=jnp.float32),
        ],
        axis=1,
    )
    reduced_high, reduced_low = split_parts(reduced)
    paired = jnp.stack([forget_cot, value_cot, gated_output], axis=1)
    upper = jnp.einsum("tkr,tkc->rkc", reduced_high, paired, preferred_element_type=jnp.float32)
    lower = jnp.einsum("tkr,tkc->rkc", reduced_low, paired, preferred_element_type=jnp.float32)
    projected = sum_at_owner(((upper + lower) * factor).astype(jnp.bfloat16), FS, 0)
    moment_one = 0.9 * first_moment + 0.1 * projected
    moment_two = 0.9 * second_moment + 0.1 * projected * projected
    direction = moment_one / (jnp.sqrt(moment_two) + 1e-08)
    piece_high, piece_low = split_parts(gather_directly(direction, FS, 0))
    upper = jnp.einsum("kdr,rkc->dkc", my_bases, piece_high, preferred_element_type=jnp.float32)
    lower = jnp.einsum("kdr,rkc->dkc", my_bases, piece_low, preferred_element_type=jnp.float32)
    full = upper + lower
    totals = over_axes(jnp.sum(direction * direction, axis=(0, 2)), FS_TP)
    entries = rank_rows * lax.axis_size(FS) * columns * lax.axis_size(TP)
    scale = lax.rsqrt(totals / entries + 1.0)
    full = full * scale[None, :, None]
    step_forget = full[:, 0, :]
    step_value = full[:, 1, :]
    step_out = full[:, 2, :].T
    new_forget = forget_weight - 0.01 * step_forget
    new_value = value_weight - 0.01 * step_value
    new_out = out_weight - 0.01 * step_out
    copy_forget, copy_value, copy_out = gather_turned(
        (
            new_forget.astype(jnp.bfloat16),
            new_value.astype(jnp.bfloat16),
            new_out.astype(jnp.bfloat16),
        ),
        FS,
        (0, 0, 1),
    )
    return (
        new_forget,
        new_value,
        new_out,
        copy_forget,
        copy_value,
        copy_out,
        moment_one,
        moment_two,
        step_forget,
        step_value,
        step_out,
    )


def solution(mesh):
    torus = Mesh(mesh.devices.reshape(4, 4, 4, 2), ("fs_0", "fs_1", "tp_0", "tp_1"))
    placed = (
        P(FS, None),
        P(FS, TP),
        P(FS, TP),
        P(FS, TP),
        P(FS, None),
        P(FS, TP),
        P(FS, TP),
        P(TP, FS),
        P(),
        P(FS, None, TP),
        P(FS, None, TP),
    )
    return jax.shard_map(
        on_device,
        mesh=torus,
        in_specs=placed,
        out_specs=(
            P(FS, TP),
            P(FS, TP),
            P(TP, FS),
            P(None, TP),
            P(None, TP),
            P(TP, None),
            P(FS, None, TP),
            P(FS, None, TP),
            P(FS, TP),
            P(FS, TP),
            P(TP, FS),
        ),
        check_vma=False,
    )
```

profile of v0, /device:TPU:1, one launch (start us, length us, event | category | flops | bytes accessed | tf_op | source)
XLA Modules:
  0.0 149.1 jit_solution(3815490610961850263)
XLA Ops:
  7.2 6.1 %convolution_bitcast_fusion.1 = f32[2048,1,256]{2,0,1:T(8,128)S(1)} fusion(bf16[2048,2048]{1,0:T(8,128)(2,1)} %param.11, bf16[3,2048,256]{2,1,0:T(8,128)(2,1)} %param.19), kind=kOutput, calls=%fused_computation.6 | convolution fusion | flops 2147483648 | bytes 11534336 | tf_op jit(solution)/shard_map/dot_general | solution.py:83
  13.3 0.9 copy-done.6
  14.2 2.5 %convolution_bitcast_fusion.2 = f32[2048,1,256]{2,0,1:T(8,128)S(1)} fusion(bf16[2048,2048]{1,0:T(8,128)(2,1)S(1)} %copy-done.6, bf16[3,2048,256]{2,1,0:T(8,128)(2,1)S(1)} %copy-done.3), kind=kOutput, calls=%fused_computation.7 | convolution fusion | flops 2147483648 | bytes 11534336 | tf_op jit(solution)/shard_map/dot_general | solution.py:82
  16.8 2.4 %convolution_bitcast_fusion = f32[2048,1,256]{2,0,1:T(8,128)S(1)} fusion(bf16[2048,2048]{1,0:T(8,128)(2,1)S(1)} %bitcast.55, bf16[3,2048,256]{2,1,0:T(8,128)(2,1)S(1)} %copy-done.3), kind=kOutput, calls=%fused_computation.5 | convolution fusion | flops 2147483648 | bytes 11534336 | tf_op jit(solution)/shard_map/dot_general | solution.py:84
  21.1 1.4 fusion.1
  22.5 1.3 fusion.5
  23.9 17.6 %all_to_all.10 = bf16[16,16,3,256]{3,1,2,0:T(8,128)(2,1)S(1)} all-to-all(bf16[16,16,3,256]{3,1,2,0:T(8,128)(2,1)S(1)} %copy.47), channel_id=1, replica_groups=mesh['fs_0'=4,'fs_1'=4,'tp_0'=4,'tp_1'=2] {'fs_0','fs_1'}, dimensions={0} | all-to-all | bytes 786432 | tf_op jit(solution)/shard_map/all_to_all | solution.py:21
  42.2 1.0 broadcast_in_dim.4
  43.2 3.6 %all-to-all-start.1 = ((f32[16,16,3,256]{3,1,2,0:T(8,128)}), f32[16,16,3,256]{3,1,2,0:T(8,128)S(1)}, u32[]{:S(2)}, u32[]{:S(2)}) async-start(f32[16,16,3,256]{3,1,2,0:T(8,128)} %broadcast_in_dim.4), calls=%async_computation.1 | async-start | bytes 1572864 | tf_op jit(solution)/shard_map/all_to_all | solution.py:33
  46.8 10.2 %psum.28 = f32[3]{0:T(128)S(1)} all-reduce(f32[3]{0:T(128)S(1)} %get-tuple-element.51), channel_id=1, replica_groups=mesh['fs_0'=4,'fs_1'=4,'tp_0'=4,'tp_1'=2] {'fs_0'}, use_global_device_ids=true, to_apply=%region_2.0 | all-reduce | flops 3 | bytes 24 | tf_op jit(solution)/shard_map/psum | solution.py:41
  57.2 12.7 %psum.29 = f32[3]{0:T(128)S(1)} all-reduce(f32[3]{0:T(128)S(1)} %psum.28), channel_id=1, replica_groups=mesh['fs_0'=4,'fs_1'=4,'tp_0'=4,'tp_1'=2] {'fs_1'}, use_global_device_ids=true, to_apply=%region_3.0 | all-reduce | flops 3 | bytes 24 | tf_op jit(solution)/shard_map/psum | solution.py:41
  70.0 8.7 %psum.30 = f32[3]{0:T(128)S(1)} all-reduce(f32[3]{0:T(128)S(1)} %psum.29), channel_id=1, replica_groups=mesh['fs_0'=4,'fs_1'=4,'tp_0'=4,'tp_1'=2] {'tp_0'}, use_global_device_ids=true, to_apply=%region_4.0 | all-reduce | flops 3 | bytes 24 | tf_op jit(solution)/shard_map/psum | solution.py:41
  78.7 7.5 %psum.31 = f32[3]{0:T(128)S(1)} all-reduce(f32[3]{0:T(128)S(1)} %psum.30), channel_id=1, replica_groups=mesh['fs_0'=4,'fs_1'=4,'tp_0'=4,'tp_1'=2] {'tp_1'}, use_global_device_ids=true, to_apply=%region_5.0 | all-reduce | flops 3 | bytes 24 | tf_op jit(solution)/shard_map/psum | solution.py:41
  86.5 1.2 fusion.16
  87.7 1.2 fusion.7
  89.0 0.7 convert_bitcast_fusion
  90.5 0.8 copy.53
  91.2 0.8 copy.54
  92.0 0.8 copy.57
  92.7 0.8 copy.58
  93.5 43.0 %all-gather.2.cloned.1.call-done = bf16[2048,768]{0,1:T(8,128)(2,1)} async-done(((bf16[128,768]{0,1:T(8,128)(2,1)}), bf16[2048,768]{0,1:T(8,128)(2,1)}) %all-gather.2.cloned.1.call-update) | async-done | bytes 3145744 | tf_op jit(solution)/shard_map/all_gather | solution.py:47
  136.5 3.1 %slice_bitcast_fusion = (bf16[256,2048]{1,0:T(8,128)(2,1)}, bf16[2048,256]{0,1:T(8,128)(2,1)S(1)}, bf16[2048,256]{0,1:T(8,128)(2,1)S(1)}) fusion(bf16[2048,768]{0,1:T(8,128)(2,1)} %all-gather.2.cloned.1.call-done), kind=kLoop, calls=%fused_computation.15 | loop fusion | bytes 6291456 | tf_op jit(solution)/shard_map/transpose | solution.py:50
  139.6 1.3 copy.55
  140.9 1.3 copy.56
  (40 shorter events, 4.0 us)
Async XLA Ops:
  7.2 6.2 %copy-start.3 = (bf16[3,2048,256]{2,1,0:T(8,128)(2,1)S(1)}, bf16[3,2048,256]{2,1,0:T(8,128)(2,1)}, u32[]{:S(2)}) copy-start(bf16[3,2048,256]{2,1,0:T(8,128)(2,1)} %param.19) | copy-start | bytes 9437188
  7.2 7.0 %copy-start.6 = (bf16[2048,2048]{1,0:T(8,128)(2,1)S(1)}, bf16[2048,2048]{1,0:T(8,128)(2,1)}, u32[]{:S(2)}) copy-start(bf16[2048,2048]{1,0:T(8,128)(2,1)} %param.11) | copy-start | bytes 25165828
  7.2 9.5 %slice-start = ((s8[8388608]{0:T(1024)(128)(4,1)}), s8[4194304]{0:T(1024)(128)(4,1)S(1)}, s32[]{:S(2)}) async-start(s8[8388608]{0:T(1024)(128)(4,1)} %bitcast.54), calls=%async_computation.3 | async-start | bytes 8388608
  14.2 2.6 %slice-start.1 = ((s8[8388608]{0:T(1024)(128)(4,1)}), s8[4194304]{0:T(1024)(128)(4,1)S(1)}, s32[]{:S(2)}) async-start(s8[8388608]{0:T(1024)(128)(4,1)} %bitcast.54), calls=%async_computation.4 | async-start | bytes 8388608
  19.2 1.2 copy-start.7
  19.2 1.5 %copy-start.8 = (bf16[2048,256]{1,0:T(8,128)(2,1)S(1)}, bf16[2048,256]{1,0:T(8,128)(2,1)}, u32[]{:S(2)}) copy-start(bf16[2048,256]{1,0:T(8,128)(2,1)} %param.13) | copy-start | bytes 3145732
  19.2 1.8 %copy-start.9 = (bf16[2048,256]{1,0:T(8,128)(2,1)S(1)}, bf16[2048,256]{1,0:T(8,128)(2,1)}, u32[]{:S(2)}) copy-start(bf16[2048,256]{1,0:T(8,128)(2,1)} %param.12) | copy-start | bytes 3145732
  22.5 19.0 %copy-start.4 = (f32[16,3,256]{2,0,1:T(8,128)S(1)}, f32[16,3,256]{2,0,1:T(8,128)}, u32[]{:S(2)}) copy-start(f32[16,3,256]{2,0,1:T(8,128)} %param.21) | copy-start | bytes 147460
  22.5 19.0 %copy-start.5 = (f32[16,3,256]{2,0,1:T(8,128)S(1)}, f32[16,3,256]{2,0,1:T(8,128)}, u32[]{:S(2)}) copy-start(f32[16,3,256]{2,0,1:T(8,128)} %param.20) | copy-start | bytes 147460
  23.8 33.3 %copy-start = (f32[128,256]{1,0:T(8,128)S(1)}, f32[128,256]{1,0:T(8,128)}, u32[]{:S(2)}) copy-start(f32[128,256]{1,0:T(8,128)} %param.16) | copy-start | bytes 393220
  23.8 46.1 %copy-start.1 = (f32[128,256]{1,0:T(8,128)S(1)}, f32[128,256]{1,0:T(8,128)}, u32[]{:S(2)}) copy-start(f32[128,256]{1,0:T(8,128)} %param.17) | copy-start | bytes 393220
  43.2 43.1 %all-to-all-start.1 = ((f32[16,16,3,256]{3,1,2,0:T(8,128)}), f32[16,16,3,256]{3,1,2,0:T(8,128)S(1)}, u32[]{:S(2)}, u32[]{:S(2)}) async-start(f32[16,16,3,256]{3,1,2,0:T(8,128)} %broadcast_in_dim.4), calls=%async_computation.1 | async-start | bytes 1572864 | tf_op jit(solution)/shard_map/all_to_all | solution.py:33
  46.8 89.7 %all-gather.2.cloned.1.call-start = ((), (), s32[]{:S(2)}) async-start(), calls=%async_computation.2 | async-start | bytes 3342336 | tf_op jit(solution)/shard_map/all_gather | solution.py:47
  86.2 2.7 %copy-start.2 = (f32[256,128]{1,0:T(8,128)S(1)}, f32[256,128]{1,0:T(8,128)}, u32[]{:S(2)}) copy-start(f32[256,128]{1,0:T(8,128)} %param.18) | copy-start | bytes 393220
Sparse Core Ops, SparseCore 0:
  90.6 45.9 all-gather.1
where the time goes:
time: 150 us; the launch traced here: 149 us
  blocking collectives  56.8 us (38%)
  waiting for transfers between devices  43 us (29%)
  matrix products  16.1 us (11%)
  between operations  14.3 us (10%)
  local copies, waits for them, and re-layouts  12.2 us (8%)
  starting transfers between devices  3.66 us (2%)
  other arithmetic  2.94 us (2%)
    all_gather x1, waiting for transfers between devices, gather_turned(): lax.all_gather(both, axis, axis=0, tiled=True)  43 us
    psum x4, blocking collectives, over_axes(): return functools.reduce(lax.psum, axes, value)  39.2 us
    all_to_all x1, blocking collectives, sum_at_owner(): lax.all_to_all(pieces, axis, split_axis=0, concat_axis=0, tiled=True)  17.6 us
    unnamed x32, local copies, waits for them, and re-layouts  8.05 us
    dot_general x1, matrix products, on_device(): jnp.dot(normed_input, bases[1], preferred_element_type=jnp.float32)  6.11 us
    all_to_all x1, starting transfers between devices, sent_to_all(): return lax.all_to_all(copies, axis, split_axis=0, concat_axis=0, tiled=True)  3.61 us
    transpose x1, local copies, waits for them, and re-layouts, gather_turned(): finished.append(jnp.moveaxis(piece, 0, dim))  3.11 us
  transfers between devices with their start and end apart: 2, of which 1 were waited for; matrix products, arithmetic and copies ran while one was open for 2% of the time, Pallas kernels for 0%

commit v1 on v0

v1 whole, which is shorter than its diff:
```python
import functools

import jax
import jax.numpy as jnp
from jax import lax
from jax.experimental import pallas as pl
from jax.experimental.pallas import tpu as pltpu
from jax.sharding import Mesh
from jax.sharding import PartitionSpec as P

FS = ("z", "x")
TP = ("y", "c")
F32 = jnp.float32
BF16 = jnp.bfloat16
RING = 4
PEERS = [(dz, dx) for dz in range(4) for dx in range(4) if (dz, dx) != (0, 0)]
TP_PEERS = [(dy, dc) for dy in range(4) for dc in range(2) if (dy, dc) != (0, 0)]
CHUNK = 256
MiB = 1 << 20


def contract(lhs, rhs, left, right):
    return lax.dot_general(lhs, rhs, (((left,), (right,)), ((), ())), preferred_element_type=F32)


def exchange(
    x_hbm, y_hbm, fc_hbm, vc_hbm, go_hbm, wf_hbm, wv_hbm, wo_hbm, b_hbm, m1_hbm, m2_hbm,
    g, dg, tot, m1o, m2o, bcat, wf, wv, wo,
    xb, yb, cots, m1b, m2b, pacc, psend, parr, s1, s2,
    wsem, bsem, msem, xsem, ysem, csem, gs, gr, a_s, a_r, d_s, d_r, t_s, t_r, u_s, u_r,
):
    at = {a: lax.axis_index(a) for a in ("z", "x", "y", "c")}
    shift = lambda a, d: lax.rem(at[a] + (d % RING), RING)
    me = at["z"] * RING + at["x"]
    tokens = xb.shape[0]
    chunks = tokens // CHUNK
    factor = float(tokens * RING * RING) ** (-0.5)

    w_copies = [
        pltpu.make_async_copy(s, d, wsem.at[i])
        for i, (s, d) in enumerate(((wf_hbm, wf), (wv_hbm, wv), (wo_hbm, wo)))
    ]
    b_copies = [
        pltpu.make_async_copy(b_hbm.at[k], bcat.at[:, 256 * k : 256 * k + 256], bsem.at[k])
        for k in range(3)
    ]
    m_copies = [
        pltpu.make_async_copy(s, d, msem.at[i]) for i, (s, d) in enumerate(((m1_hbm, m1b), (m2_hbm, m2b)))
    ]

    def rows_of(i):
        return pl.ds(pl.multiple_of(i * CHUNK, CHUNK), CHUNK)

    def x_copies(i):
        r = rows_of(i)
        return (
            pltpu.make_async_copy(x_hbm.at[r], xb.at[r], xsem.at[i]),
            pltpu.make_async_copy(fc_hbm.at[r], cots.at[0, r], csem.at[0, i]),
            pltpu.make_async_copy(vc_hbm.at[r], cots.at[1, r], csem.at[1, i]),
        )

    def y_copies(i):
        r = rows_of(i)
        return (
            pltpu.make_async_copy(y_hbm.at[r], yb.at[r], ysem.at[i]),
            pltpu.make_async_copy(go_hbm.at[r], cots.at[2, r], csem.at[2, i]),
        )

    for c in w_copies:
        c.start()
    b_copies[0].start()
    b_copies[1].start()

    @pl.loop(0, chunks)
    def _(i):
        for c in x_copies(i):
            c.start()

    b_copies[2].start()

    @pl.loop(0, chunks)
    def _(i):
        for c in y_copies(i):
            c.start()

    for c in m_copies:
        c.start()

    barrier = pltpu.get_barrier_semaphore()
    plane = [{"z": shift("z", dz), "x": shift("x", dx)} for dz, dx in PEERS]
    heads = [{"y": shift("y", dy), "c": lax.rem(at["c"] + dc, 2)} for dy, dc in TP_PEERS]
    for peer in plane + heads:
        pl.semaphore_signal(barrier, inc=1, device_id=peer)

    for c in w_copies:
        c.wait()
    for p in range(2):
        lanes = slice(128 * p, 128 * p + 128)
        g[me, 128 * p : 128 * p + 128, :] = wf[:, lanes].astype(BF16)
        g[me, 256 + 128 * p : 384 + 128 * p, :] = wv[:, lanes].astype(BF16)
    g[me, 512:768, :] = wo[...].astype(BF16)
    pacc[...] = jnp.zeros_like(pacc)
    pl.semaphore_wait(barrier, len(PEERS) + len(TP_PEERS))

    half, quarter = 384, 192

    def block(h, ja, jb):
        a, b = ("x", "z") if h == 0 else ("z", "x")
        pos = {a: shift(a, ja), b: shift(b, jb)}
        return pos["z"] * RING + pos["x"]

    def hop(h, n, ja, jb, sub, along, d):
        axis = ("x", "z")[h] if along == 0 else ("z", "x")[h]
        start, size = (half * h, half) if sub is None else (half * h + quarter * sub, quarter)

        def ref(a, b):
            return g.at[block(h, a, b), start : start + size]

        src = ref(ja, jb)
        came = ref(ja - d, jb) if along == 0 else ref(ja, jb - d)
        peer = {axis: shift(axis, d)}
        out = pltpu.make_async_remote_copy(src, src, gs.at[h, n], gr.at[h, n], device_id=peer)
        arriving = pltpu.make_async_remote_copy(came, came, gs.at[h, n], gr.at[h, n], device_id=peer)
        return out, arriving

    hops = []
    for h in range(2):
        hops.append(hop(h, 0, 0, 0, None, 0, 1))
        hops.append(hop(h, 1, 0, 0, None, 0, -1))
        hops.append(hop(h, 2, -1, 0, 0, 0, 1))
        hops.append(hop(h, 3, 1, 0, 1, 0, -1))
        for j, ja in enumerate((0, -1, 1, 2)):
            hops.append(hop(h, 4 + 4 * j, ja, 0, None, 1, 1))
            hops.append(hop(h, 5 + 4 * j, ja, 0, None, 1, -1))
            hops.append(hop(h, 6 + 4 * j, ja, -1, 0, 1, 1))
            hops.append(hop(h, 7 + 4 * j, ja, 1, 1, 1, -1))

    def send(*ids):
        for n in ids:
            for h in range(2):
                hops[20 * h + n][0].start()

    def arrive(*ids):
        for n in ids:
            for h in range(2):
                hops[20 * h + n][1].wait_recv()

    send(0, 1, 4, 5)

    b_copies[0].wait()
    b_copies[1].wait()

    def x_chunk(i):
        for c in x_copies(i):
            c.wait()
        r = rows_of(i)
        red = jnp.dot(xb[r, :], bcat[:, 0:512], preferred_element_type=F32).astype(BF16)
        pacc[0] += contract(red[:, :256], cots[0, r], 0, 0)
        pacc[1] += contract(red[:, 256:], cots[1, r], 0, 0)

    def y_chunk(i):
        for c in y_copies(i):
            c.wait()
        r = rows_of(i)
        red = jnp.dot(yb[r, :], bcat[:, 512:768], preferred_element_type=F32).astype(BF16)
        pacc[2] += contract(red, cots[2, r], 0, 0)

    pl.loop(0, chunks // 2)(x_chunk)
    pl.loop(chunks // 2, chunks)(x_chunk)
    arrive(0, 1)
    send(2, 3, 8, 9, 12, 13)

    def to_owners(ks, n):
        copies = []
        for slot, ((dz, dx), peer) in enumerate(zip(PEERS, plane)):
            owner = peer["z"] * RING + peer["x"]
            r = pl.ds(pl.multiple_of(owner * 16, 16), 16)
            copies.append(
                pltpu.make_async_remote_copy(
                    psend.at[ks, r, :], parr.at[ks, slot], a_s.at[n, slot], a_r.at[n, slot], device_id=peer
                )
            )
        return copies

    psend[0:2] = (pacc[0:2] * factor).astype(BF16)
    first = to_owners(slice(0, 2), 0)
    for c in first:
        c.start()

    b_copies[2].wait()
    pl.loop(0, chunks)(y_chunk)
    psend[2] = (pacc[2] * factor).astype(BF16)
    second = to_owners(slice(2, 3), 1)
    for c in second:
        c.start()

    arrive(4, 5)
    send(6, 7)
    arrive(2, 3)
    send(16, 17)

    for c in m_copies:
        c.wait()
    for c in first + second:
        c.wait_recv()
    mine = pl.ds(pl.multiple_of(me * 16, 16), 16)
    sums = []
    for k in range(3):
        total = psend[k, mine, :].astype(F32)
        for slot in range(len(PEERS)):
            total = total + parr[k, slot].astype(F32)
        first_moment = 0.9 * m1b[k] + 0.1 * total
        second_moment = 0.9 * m2b[k] + 0.1 * total * total
        direction = first_moment / (jnp.sqrt(second_moment) + 1e-08)
        m1o[k] = first_moment
        m2o[k] = second_moment
        dg[k, mine, :] = direction.astype(BF16)
        sums.append(jnp.sum(direction * direction))
    lane = lax.broadcasted_iota(jnp.int32, (1, 128), 1)
    row = jnp.zeros((1, 128), F32)
    for k in range(3):
        row = row + jnp.where(lane == k, sums[k], 0.0)
    s1[len(TP_PEERS)] = row
    across = [
        pltpu.make_async_remote_copy(
            s1.at[len(TP_PEERS)], s1.at[n], t_s.at[n], t_r.at[n], device_id=peer
        )
        for n, peer in enumerate(heads)
    ]
    for c in across:
        c.start()
    spread = [
        pltpu.make_async_remote_copy(
            dg.at[:, mine, :], dg.at[:, mine, :], d_s.at[n], d_r.at[n], device_id=peer
        )
        for n, peer in enumerate(plane)
    ]
    for c in spread:
        c.start()
    for c in across:
        c.wait_recv()
    s2[len(PEERS)] = jnp.sum(s1[...], axis=0)
    around = [
        pltpu.make_async_remote_copy(
            s2.at[len(PEERS)], s2.at[n], u_s.at[n], u_r.at[n], device_id=peer
        )
        for n, peer in enumerate(plane)
    ]
    for c in around:
        c.start()

    arrive(8, 9, 12, 13)
    send(10, 11, 14, 15)
    arrive(16, 17)
    send(18, 19)

    for n, ((dz, dx), peer) in enumerate(zip(PEERS, plane)):
        came = shift("z", -dz) * RING + shift("x", -dx)
        r = pl.ds(pl.multiple_of(came * 16, 16), 16)
        pltpu.make_async_remote_copy(
            dg.at[:, r, :], dg.at[:, r, :], d_s.at[n], d_r.at[n], device_id=peer
        ).wait_recv()
    for c in around:
        c.wait_recv()
    tot[...] = jnp.sum(s2[...], axis=0)
    arrive(6, 7, 10, 11, 14, 15, 18, 19)
    for out, _ in hops:
        out.wait_send()
    for c in first + second + across + spread + around:
        c.wait_send()


def finish(
    entries, g, dg, tot, m1i, m2i, bcat, wf, wv, wo,
    nf_h, nv_h, no_h, cf_h, cv_h, co_h, m1_h, m2_h, sf_h, sv_h, so_h,
    nf, nv, no, cf, cv, co, sf, sv, so, dt, sem, csem,
):
    me = lax.axis_index("z") * RING + lax.axis_index("x")
    moments = [
        pltpu.make_async_copy(m1i, m1_h, sem.at[0]),
        pltpu.make_async_copy(m2i, m2_h, sem.at[1]),
    ]
    for c in moments:
        c.start()
    row = tot[...]
    lane = lax.broadcasted_iota(jnp.int32, (1, 128), 1)
    scale = [
        lax.rsqrt(jnp.sum(jnp.where(lane == k, row, 0.0), axis=1, keepdims=True) / entries + 1.0)
        for k in range(3)
    ]
    dt[...] = dg[2].astype(F32).T.astype(BF16)
    rows = pl.ds(pl.multiple_of(me * 128, 128), 128)
    for k, (w, new, step) in enumerate(((wf, nf, sf), (wv, nv, sv))):
        full = jnp.dot(bcat[rows, 256 * k : 256 * k + 256], dg[k], preferred_element_type=F32) * scale[k]
        step[...] = full
        new[...] = w[...] - 0.01 * full
    full = contract(dt[...], bcat[rows, 512:768], 1, 1) * scale[2]
    so[...] = full
    no[...] = wo[...] - 0.01 * full
    own = [
        pltpu.make_async_copy(s, d, sem.at[2 + i])
        for i, (s, d) in enumerate(
            ((nf, nf_h), (nv, nv_h), (no, no_h), (sf, sf_h), (sv, sv_h), (so, so_h))
        )
    ]
    for c in own:
        c.start()
    outs = []
    for i in range(8):
        r = slice(256 * i, 256 * i + 256)
        for k, (copy, hbm) in enumerate(((cf, cf_h), (cv, cv_h))):
            full = jnp.dot(bcat[r, 256 * k : 256 * k + 256], dg[k], preferred_element_type=F32)
            full = full * (0.01 * scale[k])
            for b in range(2):
                for p in range(2):
                    base = 256 * k + 128 * p
                    old = g[2 * i + b, base : base + 128, :].astype(F32)
                    part = full[128 * b : 128 * b + 128, 128 * p : 128 * p + 128]
                    copy[256 * i + 128 * b : 256 * i + 128 * b + 128, 128 * p : 128 * p + 128] = (
                        old - part
                    ).astype(BF16)
            outs.append(pltpu.make_async_copy(copy.at[r], hbm.at[r], csem.at[k, i]))
            outs[-1].start()
        full = contract(dt[...], bcat[r, 512:768], 1, 1) * (0.01 * scale[2])
        for b in range(2):
            old = g[2 * i + b, 512:768, :].astype(F32)
            co[:, 256 * i + 128 * b : 256 * i + 128 * b + 128] = (
                old - full[:, 128 * b : 128 * b + 128]
            ).astype(BF16)
        outs.append(pltpu.make_async_copy(co.at[:, r], co_h.at[:, r], csem.at[2, i]))
        outs[-1].start()
    for c in moments + own + outs:
        c.wait()


def on_device(x, fc, vc, go, y, wf, wv, wo, bases, m1, m2):
    tokens = x.shape[0]
    hbm = pl.BlockSpec(memory_space=pltpu.HBM)
    vmem = pl.BlockSpec(memory_space=pltpu.VMEM)
    dma = pltpu.SemaphoreType.DMA
    m1, m2 = (jnp.transpose(m, (1, 0, 2)) for m in (m1, m2))
    args = [
        pltpu.with_memory_space_constraint(a, pltpu.HBM) for a in (x, y, fc, vc, go, wf, wv, wo, bases, m1, m2)
    ]
    held = pl.pallas_call(
        exchange,
        name="exchange",
        out_shape=[
            pltpu.VMEM((16, 768, 128), BF16),
            pltpu.VMEM((3, 256, 256), BF16),
            pltpu.VMEM((1, 128), F32),
            pltpu.VMEM((3, 16, 256), F32),
            pltpu.VMEM((3, 16, 256), F32),
            pltpu.VMEM((2048, 768), BF16),
            pltpu.VMEM((128, 256), F32),
            pltpu.VMEM((128, 256), F32),
            pltpu.VMEM((256, 128), F32),
        ],
        in_specs=[hbm] * 11,
        out_specs=[vmem] * 9,
        scratch_shapes=[
            pltpu.VMEM((tokens, 2048), BF16),
            pltpu.VMEM((tokens, 2048), BF16),
            pltpu.VMEM((3, tokens, 256), BF16),
            pltpu.VMEM((3, 16, 256), F32),
            pltpu.VMEM((3, 16, 256), F32),
            pltpu.VMEM((3, 256, 256), F32),
            pltpu.VMEM((3, 256, 256), BF16),
            pltpu.VMEM((3, 15, 16, 256), BF16),
            pltpu.VMEM((8, 1, 128), F32),
            pltpu.VMEM((16, 1, 128), F32),
            dma((3,)),
            dma((3,)),
            dma((2,)),
            dma((8,)),
            dma((8,)),
            dma((3, 8)),
            dma((2, 20)),
            dma((2, 20)),
            dma((2, 15)),
            dma((2, 15)),
            dma((15,)),
            dma((15,)),
            dma((7,)),
            dma((7,)),
            dma((15,)),
            dma((15,)),
        ],
        compiler_params=pltpu.CompilerParams(
            collective_id=0, has_side_effects=True, vmem_limit_bytes=40 * MiB
        ),
    )(*args)
    shapes = [
        ((128, 256), F32),
        ((128, 256), F32),
        ((256, 128), F32),
        ((2048, 256), BF16),
        ((2048, 256), BF16),
        ((256, 2048), BF16),
        ((3, 16, 256), F32),
        ((3, 16, 256), F32),
        ((128, 256), F32),
        ((128, 256), F32),
        ((256, 128), F32),
    ]
    outs = pl.pallas_call(
        functools.partial(finish, float(256 * 2048)),
        name="finish",
        out_shape=[jax.ShapeDtypeStruct(*s) for s in shapes],
        in_specs=[vmem] * 9,
        out_specs=[hbm] * 11,
        scratch_shapes=[
            *(pltpu.VMEM(*s) for s in shapes[:6]),
            *(pltpu.VMEM(*s) for s in shapes[8:]),
            pltpu.VMEM((256, 256), BF16),
            dma((8,)),
            dma((3, 8)),
        ],
        compiler_params=pltpu.CompilerParams(vmem_limit_bytes=24 * MiB),
    )(*held)
    outs = list(outs)
    outs[6], outs[7] = (jnp.transpose(m, (1, 0, 2)) for m in outs[6:8])
    return tuple(outs)


def solution(mesh):
    torus = Mesh(mesh.devices.reshape(4, 4, 4, 2), ("z", "x", "y", "c"))
    rows, heads, both = P(FS, None), P(FS, TP), P(FS, None, TP)
    turned = P(TP, FS)
    return jax.shard_map(
        on_device,
        mesh=torus,
        in_specs=(rows, heads, heads, heads, rows, heads, heads, turned, P(), both, both),
        out_specs=(
            heads, heads, turned, P(None, TP), P(None, TP), P(TP, None), both, both, heads, heads, turned,
        ),
        check_vma=False,
    )
```

time: 150 us -> 45.4 us (0.30)
  blocking collectives: 56.8 us -> 0 us
  Pallas kernels: 0 us -> 44.6 us
  waiting for transfers between devices: 43 us -> 0 us
  matrix products: 16.1 us -> 0 us
  between operations: 14.3 us -> 0.66 us
  local copies, waits for them, and re-layouts: 12.2 us -> 0 us
  starting transfers between devices: 3.66 us -> 0 us
  other arithmetic: 2.94 us -> 0 us
    pallas_call x0 -> x2, Pallas kernels: none -> 44.6 us  [the longest x1 42.1 us: on_device(): pl.pallas_call(exchange, name='exchange', out_shape=[pltpu.VMEM((16, 768,...]
    all_gather x1 -> x0, waiting for transfers between devices: 43 us -> none  [gather_turned(): lax.all_gather(both, axis, axis=0, tiled=True)]
    psum x4 -> x0, blocking collectives: 39.2 us -> none  [over_axes(): return functools.reduce(lax.psum, axes, value)]
    all_to_all x1 -> x0, blocking collectives: 17.6 us -> none  [sum_at_owner(): lax.all_to_all(pieces, axis, split_axis=0, concat_axis=0, tiled=True)]
    dot_general x7 -> x0, matrix products: 16.1 us -> none  [the longest x1 6.11 us: on_device(): jnp.dot(normed_input, bases[1], preferred_element_type=jnp.float32)]
    unnamed x32 -> x0, local copies, waits for them, and re-layouts: 8.05 us -> none
    all_to_all x1 -> x0, starting transfers between devices: 3.61 us -> none  [sent_to_all(): return lax.all_to_all(copies, axis, split_axis=0, concat_axis=0, tiled=True)]
    transpose x1 -> x0, local copies, waits for them, and re-layouts: 3.11 us -> none  [gather_turned(): finished.append(jnp.moveaxis(piece, 0, dim))]
  transfers between devices with their start and end apart: 2 -> 0, of which waited for: 1 -> 0; matrix products, arithmetic and copies ran while one was open for 2% -> 0% of each run, Pallas kernels for 0% -> 0%
where the time goes in v1:
time: 45.4 us; the launch traced here: 45.3 us
  Pallas kernels  44.6 us (98%)
  between operations  0.66 us (1%)
    pallas_call x1, Pallas kernels, on_device(): pl.pallas_call(exchange, name='exchange', out_shape=[pltpu.VMEM((16, 768,...  42.1 us
    pallas_call x1, Pallas kernels, on_device(): pl.pallas_call(functools.partial(finish, float(256 * 2048)), name='finish...  2.52 us

profile of v1, /device:TPU:1, one launch (start us, length us, event | category | flops | bytes accessed | tf_op | source)
XLA Modules:
  0.0 45.3 jit_solution(16059466538091802678)
XLA Ops:
  0.6 42.1 %exchange.1 = (bf16[16,768,128]{2,1,0:T(8,128)(2,1)S(1)}, bf16[3,256,256]{2,1,0:T(8,128)(2,1)S(1)}, f32[1,128]{1,0:T(1,128)S(1)}, f32[3,16,256]{2,1,0:T(8,128)S(...) custom-call(bf16[2048,2048]{1,0:T(8,128)(2,1)} %x_hbm.1, ...), custom_call_target="tpu_custom_call" | custom-call | tf_op jit(solution)/shard_map/exchange/pallas_call | solution.py:345
  42.8 2.5 %finish.1 = (f32[128,256]{1,0:T(8,128)}, f32[128,256]{1,0:T(8,128)}, f32[256,128]{1,0:T(8,128)}, bf16[2048,256]{1,0:T(8,128)(2,1)}, bf16[2048,256]{1,0:T(8,128)(...) custom-call(bf16[16,768,128]{2,1,0:T(8,128)(2,1)S(1)} %get-tuple-ele, ...), custom_call_target="tpu_custom_call" | custom-call | tf_op jit(solution)/shard_map/finish/pallas_call | solution.py:406

commit v2 on v1

--- a/solution.py
+++ b/solution.py
@@ -13,9 +13,11 @@
 F32 = jnp.float32
 BF16 = jnp.bfloat16
 RING = 4
+HOPS = (1, 2, 3)
 PEERS = [(dz, dx) for dz in range(4) for dx in range(4) if (dz, dx) != (0, 0)]
+AXES = (("x", "z"), ("z", "x"))
 TP_PEERS = [(dy, dc) for dy in range(4) for dc in range(2) if (dy, dc) != (0, 0)]
-CHUNK = 256
+CHUNK = 512
 MiB = 1 << 20
 
 
@@ -26,15 +28,18 @@
 def exchange(
     x_hbm, y_hbm, fc_hbm, vc_hbm, go_hbm, wf_hbm, wv_hbm, wo_hbm, b_hbm, m1_hbm, m2_hbm,
     g, dg, tot, m1o, m2o, bcat, wf, wv, wo,
-    xb, yb, cots, m1b, m2b, pacc, psend, parr, s1, s2,
-    wsem, bsem, msem, xsem, ysem, csem, gs, gr, a_s, a_r, d_s, d_r, t_s, t_r, u_s, u_r,
+    xb, yb, cots, red, m1b, m2b, pacc, psend, parr, s1, s2,
+    wsem, bsem, msem, xsem, ysem, csem, r_s, r_r, gs, gr, a_s, a_r, d_s, d_r, e_s, e_r, t_s, t_r, u_s, u_r,
 ):
     at = {a: lax.axis_index(a) for a in ("z", "x", "y", "c")}
     shift = lambda a, d: lax.rem(at[a] + (d % RING), RING)
     me = at["z"] * RING + at["x"]
-    tokens = xb.shape[0]
-    chunks = tokens // CHUNK
+    half_tokens = xb.shape[0]
+    tokens = 2 * half_tokens
+    chunks = half_tokens // CHUNK
     factor = float(tokens * RING * RING) ** (-0.5)
+    mine_from = at["c"] * half_tokens
+    other_from = half_tokens - mine_from
 
     w_copies = [
         pltpu.make_async_copy(s, d, wsem.at[i])
@@ -48,50 +53,31 @@
         pltpu.make_async_copy(s, d, msem.at[i]) for i, (s, d) in enumerate(((m1_hbm, m1b), (m2_hbm, m2b)))
     ]
 
-    def rows_of(i):
-        return pl.ds(pl.multiple_of(i * CHUNK, CHUNK), CHUNK)
-
-    def x_copies(i):
-        r = rows_of(i)
-        return (
-            pltpu.make_async_copy(x_hbm.at[r], xb.at[r], xsem.at[i]),
-            pltpu.make_async_copy(fc_hbm.at[r], cots.at[0, r], csem.at[0, i]),
-            pltpu.make_async_copy(vc_hbm.at[r], cots.at[1, r], csem.at[1, i]),
-        )
-
-    def y_copies(i):
-        r = rows_of(i)
-        return (
-            pltpu.make_async_copy(y_hbm.at[r], yb.at[r], ysem.at[i]),
-            pltpu.make_async_copy(go_hbm.at[r], cots.at[2, r], csem.at[2, i]),
-        )
-
-    for c in w_copies:
-        c.start()
-    b_copies[0].start()
-    b_copies[1].start()
-
-    @pl.loop(0, chunks)
-    def _(i):
-        for c in x_copies(i):
-            c.start()
-
-    b_copies[2].start()
-
-    @pl.loop(0, chunks)
-    def _(i):
-        for c in y_copies(i):
-            c.start()
-
-    for c in m_copies:
-        c.start()
+    def in_array(i):
+        return pl.ds(pl.multiple_of(mine_from + i * CHUNK, CHUNK), CHUNK)
+
+    def in_half(i):
+        return slice(i * CHUNK, i * CHUNK + CHUNK)
+
+    x_copies = [
+        pltpu.make_async_copy(x_hbm.at[in_array(i)], xb.at[in_half(i)], xsem.at[i]) for i in range(chunks)
+    ]
+    y_copies = [
+        pltpu.make_async_copy(y_hbm.at[in_array(i)], yb.at[in_half(i)], ysem.at[i]) for i in range(chunks)
+    ]
+    c_copies = [
+        pltpu.make_async_copy(s, cots.at[k], csem.at[k]) for k, s in enumerate((fc_hbm, vc_hbm, go_hbm))
+    ]
 
     barrier = pltpu.get_barrier_semaphore()
     plane = [{"z": shift("z", dz), "x": shift("x", dx)} for dz, dx in PEERS]
+    ring = {a: [{a: shift(a, d)} for d in HOPS] for a in ("x", "z")}
     heads = [{"y": shift("y", dy), "c": lax.rem(at["c"] + dc, 2)} for dy, dc in TP_PEERS]
     for peer in plane + heads:
         pl.semaphore_signal(barrier, inc=1, device_id=peer)
 
+    for c in w_copies + b_copies[:2] + x_copies:
+        c.start()
     for c in w_copies:
         c.wait()
     for p in range(2):
@@ -99,8 +85,35 @@
         g[me, 128 * p : 128 * p + 128, :] = wf[:, lanes].astype(BF16)
         g[me, 256 + 128 * p : 384 + 128 * p, :] = wv[:, lanes].astype(BF16)
     g[me, 512:768, :] = wo[...].astype(BF16)
-    pacc[...] = jnp.zeros_like(pacc)
     pl.semaphore_wait(barrier, len(PEERS) + len(TP_PEERS))
+
+    def reduce_x(i):
+        red[in_array(i), 0:512] = jnp.dot(
+            xb[in_half(i), :], bcat[:, 0:512], preferred_element_type=F32
+        ).astype(BF16)
+
+    def reduce_y(i):
+        red[in_array(i), 512:768] = jnp.dot(
+            yb[in_half(i), :], bcat[:, 512:768], preferred_element_type=F32
+        ).astype(BF16)
+
+    mine_rows = pl.ds(pl.multiple_of(mine_from, CHUNK), half_tokens)
+    other_rows = pl.ds(pl.multiple_of(other_from, CHUNK), half_tokens)
+    partner = {"c": 1 - at["c"]}
+
+    def shared(rows, lanes, n):
+        ref = red.at[rows, lanes]
+        return pltpu.make_async_remote_copy(ref, ref, r_s.at[n], r_r.at[n], device_id=partner)
+
+    x_part, y_part = slice(0, 512), slice(512, 768)
+    in_other = [pl.ds(pl.multiple_of(other_from + i * CHUNK, CHUNK), CHUNK) for i in range(chunks)]
+    over, back = (
+        [shared(part(i), lanes, chunks * n + i) for n, lanes in enumerate((x_part, y_part)) for i in range(chunks)]
+        for part in (in_array, lambda i: in_other[i])
+    )
+
+    def project(k, rows):
+        return contract(red[rows, 256 * k : 256 * k + 256], cots[k, rows], 0, 0)
 
     half, quarter = 384, 192
 
@@ -147,32 +160,25 @@
 
     send(0, 1, 4, 5)
 
-    b_copies[0].wait()
-    b_copies[1].wait()
-
-    def x_chunk(i):
-        for c in x_copies(i):
-            c.wait()
-        r = rows_of(i)
-        red = jnp.dot(xb[r, :], bcat[:, 0:512], preferred_element_type=F32).astype(BF16)
-        pacc[0] += contract(red[:, :256], cots[0, r], 0, 0)
-        pacc[1] += contract(red[:, 256:], cots[1, r], 0, 0)
-
-    def y_chunk(i):
-        for c in y_copies(i):
-            c.wait()
-        r = rows_of(i)
-        red = jnp.dot(yb[r, :], bcat[:, 512:768], preferred_element_type=F32).astype(BF16)
-        pacc[2] += contract(red, cots[2, r], 0, 0)
-
-    pl.loop(0, chunks // 2)(x_chunk)
-    pl.loop(chunks // 2, chunks)(x_chunk)
-    arrive(0, 1)
-    send(2, 3, 8, 9, 12, 13)
+    for c in b_copies[:2]:
+        c.wait()
+    x_copies[0].wait()
+    for c in b_copies[2:] + y_copies + c_copies + m_copies:
+        c.start()
+    reduce_x(0)
+    over[0].start()
+    x_copies[1].wait()
+    reduce_x(1)
+    over[1].start()
+
+    for c in c_copies[:2]:
+        c.wait()
+    for k in range(2):
+        pacc[k] = project(k, mine_rows)
 
     def to_owners(ks, n):
         copies = []
-        for slot, ((dz, dx), peer) in enumerate(zip(PEERS, plane)):
+        for slot, peer in enumerate(plane):
             owner = peer["z"] * RING + peer["x"]
             r = pl.ds(pl.multiple_of(owner * 16, 16), 16)
             copies.append(
@@ -182,29 +188,39 @@
             )
         return copies
 
-    psend[0:2] = (pacc[0:2] * factor).astype(BF16)
+    back[0].wait_recv()
+    back[1].wait_recv()
+    for k in range(2):
+        psend[k] = ((pacc[k] + project(k, other_rows)) * factor).astype(BF16)
     first = to_owners(slice(0, 2), 0)
     for c in first:
         c.start()
 
     b_copies[2].wait()
-    pl.loop(0, chunks)(y_chunk)
-    psend[2] = (pacc[2] * factor).astype(BF16)
+    y_copies[0].wait()
+    reduce_y(0)
+    over[2].start()
+    y_copies[1].wait()
+    reduce_y(1)
+    over[3].start()
+    c_copies[2].wait()
+    pacc[2] = project(2, mine_rows)
+    arrive(0, 1)
+    send(2, 3)
+    back[2].wait_recv()
+    back[3].wait_recv()
+    psend[2] = ((pacc[2] + project(2, other_rows)) * factor).astype(BF16)
     second = to_owners(slice(2, 3), 1)
     for c in second:
         c.start()
 
-    arrive(4, 5)
-    send(6, 7)
-    arrive(2, 3)
-    send(16, 17)
-
+    send(8, 9, 12, 13)
     for c in m_copies:
         c.wait()
     for c in first + second:
         c.wait_recv()
     mine = pl.ds(pl.multiple_of(me * 16, 16), 16)
-    sums = []
+    squares = []
     for k in range(3):
         total = psend[k, mine, :].astype(F32)
         for slot in range(len(PEERS)):
@@ -214,66 +230,96 @@
         direction = first_moment / (jnp.sqrt(second_moment) + 1e-08)
         m1o[k] = first_moment
         m2o[k] = second_moment
-        dg[k, mine, :] = direction.astype(BF16)
-        sums.append(jnp.sum(direction * direction))
+        for h in range(2):
+            dg[h, k, at["z"], at["x"]] = direction[:, 128 * h : 128 * h + 128].astype(BF16)
+        squares.append(direction * direction)
+
+    def spread_copies(h, axis, where, sems):
+        copies, arriving = [], []
+        for i, (d, peer) in enumerate(zip(HOPS, ring[axis])):
+            src, came = where(at[axis]), where(shift(axis, -d))
+            copies.append(
+                pltpu.make_async_remote_copy(src, src, sems[0].at[h, i], sems[1].at[h, i], device_id=peer)
+            )
+            arriving.append(
+                pltpu.make_async_remote_copy(came, came, sems[0].at[h, i], sems[1].at[h, i], device_id=peer)
+            )
+        return copies, arriving
+
+    near = [
+        spread_copies(0, "x", lambda x: dg.at[0, :, at["z"], x], (d_s, d_r)),
+        spread_copies(1, "z", lambda z: dg.at[1, :, z, at["x"]], (d_s, d_r)),
+    ]
+    far = [
+        spread_copies(0, "z", lambda z: dg.at[0, :, z], (e_s, e_r)),
+        spread_copies(1, "x", lambda x: dg.at[1, :, :, x], (e_s, e_r)),
+    ]
+    for copies, _ in near:
+        for c in copies:
+            c.start()
+
+    sums = [jnp.sum(v) for v in squares]
     lane = lax.broadcasted_iota(jnp.int32, (1, 128), 1)
     row = jnp.zeros((1, 128), F32)
     for k in range(3):
         row = row + jnp.where(lane == k, sums[k], 0.0)
+
+    def sum_copies(held, peers, send_sems, recv_sems):
+        return [
+            pltpu.make_async_remote_copy(
+                held.at[len(peers)], held.at[n], send_sems.at[n], recv_sems.at[n], device_id=peer
+            )
+            for n, peer in enumerate(peers)
+        ]
+
+    across = sum_copies(s1, heads, t_s, t_r)
+    around = sum_copies(s2, plane, u_s, u_r)
     s1[len(TP_PEERS)] = row
-    across = [
-        pltpu.make_async_remote_copy(
-            s1.at[len(TP_PEERS)], s1.at[n], t_s.at[n], t_r.at[n], device_id=peer
-        )
-        for n, peer in enumerate(heads)
-    ]
     for c in across:
         c.start()
-    spread = [
-        pltpu.make_async_remote_copy(
-            dg.at[:, mine, :], dg.at[:, mine, :], d_s.at[n], d_r.at[n], device_id=peer
-        )
-        for n, peer in enumerate(plane)
-    ]
-    for c in spread:
-        c.start()
+
+    arrive(4, 5)
+    send(6, 7)
+    arrive(2, 3)
+    send(16, 17)
+
     for c in across:
         c.wait_recv()
     s2[len(PEERS)] = jnp.sum(s1[...], axis=0)
-    around = [
-        pltpu.make_async_remote_copy(
-            s2.at[len(PEERS)], s2.at[n], u_s.at[n], u_r.at[n], device_id=peer
-        )
-        for n, peer in enumerate(plane)
-    ]
     for c in around:
         c.start()
+    for _, arriving in near:
+        for c in arriving:
+            c.wait_recv()
+    for copies, _ in far:
+        for c in copies:
+            c.start()
 
     arrive(8, 9, 12, 13)
     send(10, 11, 14, 15)
     arrive(16, 17)
     send(18, 19)
 
-    for n, ((dz, dx), peer) in enumerate(zip(PEERS, plane)):
-        came = shift("z", -dz) * RING + shift("x", -dx)
-        r = pl.ds(pl.multiple_of(came * 16, 16), 16)
-        pltpu.make_async_remote_copy(
-            dg.at[:, r, :], dg.at[:, r, :], d_s.at[n], d_r.at[n], device_id=peer
-        ).wait_recv()
+    for _, arriving in far:
+        for c in arriving:
+            c.wait_recv()
     for c in around:
         c.wait_recv()
     tot[...] = jnp.sum(s2[...], axis=0)
     arrive(6, 7, 10, 11, 14, 15, 18, 19)
     for out, _ in hops:
         out.wait_send()
-    for c in first + second + across + spread + around:
+    sent = over + first + second + across + around
+    for copies, _ in near + far:
+        sent = sent + copies
+    for c in sent:
         c.wait_send()
 
 
 def finish(
     entries, g, dg, tot, m1i, m2i, bcat, wf, wv, wo,
     nf_h, nv_h, no_h, cf_h, cv_h, co_h, m1_h, m2_h, sf_h, sv_h, so_h,
-    nf, nv, no, cf, cv, co, sf, sv, so, dt, sem, csem,
+    nf, nv, no, cf, cv, co, sf, sv, so, dirs, dt, sem, csem,
 ):
     me = lax.axis_index("z") * RING + lax.axis_index("x")
     moments = [
@@ -288,10 +334,13 @@
         lax.rsqrt(jnp.sum(jnp.where(lane == k, row, 0.0), axis=1, keepdims=True) / entries + 1.0)
         for k in range(3)
     ]
-    dt[...] = dg[2].astype(F32).T.astype(BF16)
+    for k in range(3):
+        for h in range(2):
+            dirs[k, :, 128 * h : 128 * h + 128] = dg[h, k].reshape(256, 128)
+    dt[...] = dirs[2].astype(F32).T.astype(BF16)
     rows = pl.ds(pl.multiple_of(me * 128, 128), 128)
     for k, (w, new, step) in enumerate(((wf, nf, sf), (wv, nv, sv))):
-        full = jnp.dot(bcat[rows, 256 * k : 256 * k + 256], dg[k], preferred_element_type=F32) * scale[k]
+        full = jnp.dot(bcat[rows, 256 * k : 256 * k + 256], dirs[k], preferred_element_type=F32) * scale[k]
         step[...] = full
         new[...] = w[...] - 0.01 * full
     full = contract(dt[...], bcat[rows, 512:768], 1, 1) * scale[2]
@@ -309,7 +358,7 @@
     for i in range(8):
         r = slice(256 * i, 256 * i + 256)
         for k, (copy, hbm) in enumerate(((cf, cf_h), (cv, cv_h))):
-            full = jnp.dot(bcat[r, 256 * k : 256 * k + 256], dg[k], preferred_element_type=F32)
+            full = jnp.dot(bcat[r, 256 * k : 256 * k + 256], dirs[k], preferred_element_type=F32)
             full = full * (0.01 * scale[k])
             for b in range(2):
                 for p in range(2):
@@ -347,7 +396,7 @@
         name="exchange",
         out_shape=[
             pltpu.VMEM((16, 768, 128), BF16),
-            pltpu.VMEM((3, 256, 256), BF16),
+            pltpu.VMEM((2, 3, 4, 4, 16, 128), BF16),
             pltpu.VMEM((1, 128), F32),
             pltpu.VMEM((3, 16, 256), F32),
             pltpu.VMEM((3, 16, 256), F32),
@@ -359,9 +408,10 @@
         in_specs=[hbm] * 11,
         out_specs=[vmem] * 9,
         scratch_shapes=[
-            pltpu.VMEM((tokens, 2048), BF16),
-            pltpu.VMEM((tokens, 2048), BF16),
+            pltpu.VMEM((tokens // 2, 2048), BF16),
+            pltpu.VMEM((tokens // 2, 2048), BF16),
             pltpu.VMEM((3, tokens, 256), BF16),
+            pltpu.VMEM((tokens, 768), BF16),
             pltpu.VMEM((3, 16, 256), F32),
             pltpu.VMEM((3, 16, 256), F32),
             pltpu.VMEM((3, 256, 256), F32),
@@ -372,15 +422,19 @@
             dma((3,)),
             dma((3,)),
             dma((2,)),
-            dma((8,)),
-            dma((8,)),
-            dma((3, 8)),
+            dma((2,)),
+            dma((2,)),
+            dma((3,)),
+            dma((4,)),
+            dma((4,)),
             dma((2, 20)),
             dma((2, 20)),
             dma((2, 15)),
             dma((2, 15)),
-            dma((15,)),
-            dma((15,)),
+            dma((2, 3)),
+            dma((2, 3)),
+            dma((2, 3)),
+            dma((2, 3)),
             dma((7,)),
             dma((7,)),
             dma((15,)),
@@ -412,6 +466,7 @@
         scratch_shapes=[
             *(pltpu.VMEM(*s) for s in shapes[:6]),
             *(pltpu.VMEM(*s) for s in shapes[8:]),
+            pltpu.VMEM((3, 256, 256), BF16),
             pltpu.VMEM((256, 256), BF16),
             dma((8,)),
             dma((3, 8)),

time: 45.4 us -> 39.9 us (0.88)
  Pallas kernels: 44.6 us -> 39.1 us
    pallas_call x1, Pallas kernels: 42.1 us -> 36.6 us  [on_device(): pl.pallas_call(exchange, name='exchange', out_shape=[pltpu.VMEM((16, 768,...]
where the time goes in v2:
time: 39.9 us; the launch traced here: 39.8 us
  Pallas kernels  39.1 us (98%)
  between operations  0.66 us (2%)
    pallas_call x1, Pallas kernels, on_device(): pl.pallas_call(exchange, name='exchange', out_shape=[pltpu.VMEM((16, 768,...  36.6 us
    pallas_call x1, Pallas kernels, on_device(): pl.pallas_call(functools.partial(finish, float(256 * 2048)), name='finish...  2.58 us

profile of v2, /device:TPU:1, one launch (start us, length us, event | category | flops | bytes accessed | tf_op | source)
XLA Modules:
  0.0 39.8 jit_solution(3142367874118667570)
XLA Ops:
  0.6 36.6 %exchange.1 = (bf16[16,768,128]{2,1,0:T(8,128)(2,1)S(1)}, bf16[2,3,4,4,16,128]{5,4,3,2,1,0:T(8,128)(2,1)S(1)}, f32[1,128]{1,0:T(1,128)S(1)}, f32[3,16,256]{2,1,0...) custom-call(bf16[2048,2048]{1,0:T(8,128)(2,1)} %x_hbm.1, ...), custom_call_target="tpu_custom_call" | custom-call | tf_op jit(solution)/shard_map/exchange/pallas_call | solution.py:394
  37.2 2.6 %finish.1 = (f32[128,256]{1,0:T(8,128)}, f32[128,256]{1,0:T(8,128)}, f32[256,128]{1,0:T(8,128)}, bf16[2048,256]{1,0:T(8,128)(2,1)}, bf16[2048,256]{1,0:T(8,128)(...) custom-call(bf16[16,768,128]{2,1,0:T(8,128)(2,1)S(1)} %get-tuple-ele, ...), custom_call_target="tpu_custom_call" | custom-call | tf_op jit(solution)/shard_map/finish/pallas_call | solution.py:460

commit v3 on v2

--- a/solution.py
+++ b/solution.py
@@ -14,9 +14,9 @@
 BF16 = jnp.bfloat16
 RING = 4
 HOPS = (1, 2, 3)
-PEERS = [(dz, dx) for dz in range(4) for dx in range(4) if (dz, dx) != (0, 0)]
+PEERS = [(dz, dx) for dz in (2, 1, 3, 0) for dx in (2, 1, 3, 0) if (dz, dx) != (0, 0)]
 AXES = (("x", "z"), ("z", "x"))
-TP_PEERS = [(dy, dc) for dy in range(4) for dc in range(2) if (dy, dc) != (0, 0)]
+TP_PEERS = [(dy, dc) for dy in (2, 1, 3, 0) for dc in (1, 0) if (dy, dc) != (0, 0)]
 CHUNK = 512
 MiB = 1 << 20
 
@@ -69,6 +69,8 @@
         pltpu.make_async_copy(s, cots.at[k], csem.at[k]) for k, s in enumerate((fc_hbm, vc_hbm, go_hbm))
     ]
 
+    for c in w_copies:
+        c.start()
     barrier = pltpu.get_barrier_semaphore()
     plane = [{"z": shift("z", dz), "x": shift("x", dx)} for dz, dx in PEERS]
     ring = {a: [{a: shift(a, d)} for d in HOPS] for a in ("x", "z")}
@@ -76,7 +78,7 @@
     for peer in plane + heads:
         pl.semaphore_signal(barrier, inc=1, device_id=peer)
 
-    for c in w_copies + b_copies[:2] + x_copies:
+    for c in b_copies[:2] + x_copies:
         c.start()
     for c in w_copies:
         c.wait()
@@ -90,11 +92,6 @@
     def reduce_x(i):
         red[in_array(i), 0:512] = jnp.dot(
             xb[in_half(i), :], bcat[:, 0:512], preferred_element_type=F32
-        ).astype(BF16)
-
-    def reduce_y(i):
-        red[in_array(i), 512:768] = jnp.dot(
-            yb[in_half(i), :], bcat[:, 512:768], preferred_element_type=F32
         ).astype(BF16)
 
     mine_rows = pl.ds(pl.multiple_of(mine_from, CHUNK), half_tokens)
@@ -197,11 +194,10 @@
         c.start()
 
     b_copies[2].wait()
-    y_copies[0].wait()
-    reduce_y(0)
+    for c in y_copies:
+        c.wait()
+    red[mine_rows, 512:768] = jnp.dot(yb[...], bcat[:, 512:768], preferred_element_type=F32).astype(BF16)
     over[2].start()
-    y_copies[1].wait()
-    reduce_y(1)
     over[3].start()
     c_copies[2].wait()
     pacc[2] = project(2, mine_rows)
@@ -278,22 +274,22 @@
     for c in across:
         c.start()
 
+    arrive(2, 3)
+    send(16, 17)
     arrive(4, 5)
     send(6, 7)
-    arrive(2, 3)
-    send(16, 17)
-
-    for c in across:
-        c.wait_recv()
-    s2[len(PEERS)] = jnp.sum(s1[...], axis=0)
-    for c in around:
-        c.start()
+
     for _, arriving in near:
         for c in arriving:
             c.wait_recv()
     for copies, _ in far:
         for c in copies:
             c.start()
+    for c in across:
+        c.wait_recv()
+    s2[len(PEERS)] = jnp.sum(s1[...], axis=0)
+    for c in around:
+        c.start()
 
     arrive(8, 9, 12, 13)
     send(10, 11, 14, 15)

time: 39.9 us -> 38.6 us (0.967)
  Pallas kernels: 39.1 us -> 37.8 us
    pallas_call x1, Pallas kernels: 36.6 us -> 35.3 us  [on_device(): pl.pallas_call(exchange, name='exchange', out_shape=[pltpu.VMEM((16, 768,...]
where the time goes in v3:
time: 38.6 us; the launch traced here: 38.5 us
  Pallas kernels  37.8 us (98%)
  between operations  0.66 us (2%)
    pallas_call x1, Pallas kernels, on_device(): pl.pallas_call(exchange, name='exchange', out_shape=[pltpu.VMEM((16, 768,...  35.3 us
    pallas_call x1, Pallas kernels, on_device(): pl.pallas_call(functools.partial(finish, float(256 * 2048)), name='finish...  2.58 us

profile of v3, /device:TPU:1, one launch (start us, length us, event | category | flops | bytes accessed | tf_op | source)
XLA Modules:
  0.0 38.5 jit_solution(8694452670865177766)
XLA Ops:
  0.6 35.3 %exchange.1 = (bf16[16,768,128]{2,1,0:T(8,128)(2,1)S(1)}, bf16[2,3,4,4,16,128]{5,4,3,2,1,0:T(8,128)(2,1)S(1)}, f32[1,128]{1,0:T(1,128)S(1)}, f32[3,16,256]{2,1,0...) custom-call(bf16[2048,2048]{1,0:T(8,128)(2,1)} %x_hbm.1, ...), custom_call_target="tpu_custom_call" | custom-call | tf_op jit(solution)/shard_map/exchange/pallas_call | solution.py:390
  35.9 2.6 %finish.1 = (f32[128,256]{1,0:T(8,128)}, f32[128,256]{1,0:T(8,128)}, f32[256,128]{1,0:T(8,128)}, bf16[2048,256]{1,0:T(8,128)(2,1)}, bf16[2048,256]{1,0:T(8,128)(...) custom-call(bf16[16,768,128]{2,1,0:T(8,128)(2,1)S(1)} %get-tuple-ele, ...), custom_call_target="tpu_custom_call" | custom-call | tf_op jit(solution)/shard_map/finish/pallas_call | solution.py:456

commit v4 on v3

--- a/solution.py
+++ b/solution.py
@@ -250,9 +250,9 @@
         spread_copies(0, "z", lambda z: dg.at[0, :, z], (e_s, e_r)),
         spread_copies(1, "x", lambda x: dg.at[1, :, :, x], (e_s, e_r)),
     ]
-    for copies, _ in near:
-        for c in copies:
-            c.start()
+    for n in (1, 0, 2):
+        for copies, _ in near:
+            copies[n].start()
 
     sums = [jnp.sum(v) for v in squares]
     lane = lax.broadcasted_iota(jnp.int32, (1, 128), 1)
@@ -334,22 +334,6 @@
         for h in range(2):
             dirs[k, :, 128 * h : 128 * h + 128] = dg[h, k].reshape(256, 128)
     dt[...] = dirs[2].astype(F32).T.astype(BF16)
-    rows = pl.ds(pl.multiple_of(me * 128, 128), 128)
-    for k, (w, new, step) in enumerate(((wf, nf, sf), (wv, nv, sv))):
-        full = jnp.dot(bcat[rows, 256 * k : 256 * k + 256], dirs[k], preferred_element_type=F32) * scale[k]
-        step[...] = full
-        new[...] = w[...] - 0.01 * full
-    full = contract(dt[...], bcat[rows, 512:768], 1, 1) * scale[2]
-    so[...] = full
-    no[...] = wo[...] - 0.01 * full
-    own = [
-        pltpu.make_async_copy(s, d, sem.at[2 + i])
-        for i, (s, d) in enumerate(
-            ((nf, nf_h), (nv, nv_h), (no, no_h), (sf, sf_h), (sv, sv_h), (so, so_h))
-        )
-    ]
-    for c in own:
-        c.start()
     outs = []
     for i in range(8):
         r = slice(256 * i, 256 * i + 256)
@@ -374,6 +358,22 @@
             ).astype(BF16)
         outs.append(pltpu.make_async_copy(co.at[:, r], co_h.at[:, r], csem.at[2, i]))
         outs[-1].start()
+    rows = pl.ds(pl.multiple_of(me * 128, 128), 128)
+    for k, (w, new, step) in enumerate(((wf, nf, sf), (wv, nv, sv))):
+        full = jnp.dot(bcat[rows, 256 * k : 256 * k + 256], dirs[k], preferred_element_type=F32) * scale[k]
+        step[...] = full
+        new[...] = w[...] - 0.01 * full
+    full = contract(dt[...], bcat[rows, 512:768], 1, 1) * scale[2]
+    so[...] = full
+    no[...] = wo[...] - 0.01 * full
+    own = [
+        pltpu.make_async_copy(s, d, sem.at[2 + i])
+        for i, (s, d) in enumerate(
+            ((nf, nf_h), (nv, nv_h), (no, no_h), (sf, sf_h), (sv, sv_h), (so, so_h))
+        )
+    ]
+    for c in own:
+        c.start()
     for c in moments + own + outs:
         c.wait()
 

time: 38.6 us -> 38.6 us (level)
  no operation moved by 1% of the time
where the time goes in v4:
time: 38.6 us; the launch traced here: 38.5 us
  Pallas kernels  37.8 us (98%)
  between operations  0.66 us (2%)
    pallas_call x1, Pallas kernels, on_device(): pl.pallas_call(exchange, name='exchange', out_shape=[pltpu.VMEM((16, 768,...  35.3 us
    pallas_call x1, Pallas kernels, on_device(): pl.pallas_call(functools.partial(finish, float(256 * 2048)), name='finish...  2.57 us

profile of v4, /device:TPU:1, one launch (start us, length us, event | category | flops | bytes accessed | tf_op | source)
XLA Modules:
  0.0 38.5 jit_solution(803839405560683975)
XLA Ops:
  0.6 35.3 %exchange.1 = (bf16[16,768,128]{2,1,0:T(8,128)(2,1)S(1)}, bf16[2,3,4,4,16,128]{5,4,3,2,1,0:T(8,128)(2,1)S(1)}, f32[1,128]{1,0:T(1,128)S(1)}, f32[3,16,256]{2,1,0...) custom-call(bf16[2048,2048]{1,0:T(8,128)(2,1)} %x_hbm.1, ...), custom_call_target="tpu_custom_call" | custom-call | tf_op jit(solution)/shard_map/exchange/pallas_call | solution.py:390
  35.9 2.6 %finish.1 = (f32[128,256]{1,0:T(8,128)}, f32[128,256]{1,0:T(8,128)}, f32[256,128]{1,0:T(8,128)}, bf16[2048,256]{1,0:T(8,128)(2,1)}, bf16[2048,256]{1,0:T(8,128)(...) custom-call(bf16[16,768,128]{2,1,0:T(8,128)(2,1)S(1)} %get-tuple-ele, ...), custom_call_target="tpu_custom_call" | custom-call | tf_op jit(solution)/shard_map/finish/pallas_call | solution.py:456
